TPU v7x, 768 devices: a whole 4x8x12 slice. The times are simulated.
768 devices in a mesh: gr: 3 (over z_hi), sp: 32 (over z_lo, y), tp: 8 (over x, core).
Axes of the slice: x: 4, y: 8, z: 12 (z_hi: 3, z_lo: 4; z = z_hi * 4 + z_lo), core: 2. Of those that a mesh axis runs over, the one named last changes fastest.
Arguments:
- tokens: bfloat16 [12, 6144, 4096], P('gr', 'sp'), parts along dimension 0, may hold values from -50 to 50
- new_tokens: bfloat16 [12, 4096], P('gr'), parts along dimension 0, may hold values from -6 to 6
- in_gain: float32 [4096], replicated, may hold values from 0.1 to 1.9
- w_forget: bfloat16 [4096, 2048], P(None, 'tp'), may hold values from -0.09375 to 0.09375
- w_value: bfloat16 [4096, 2048], P(None, 'tp'), may hold values from -0.75 to 0.75
- gap: float32 [16, 128], P('tp'), may hold values from 0 to 0.06
- decay_shift: float32 [12, 6144, 16], P('gr', 'sp', 'tp'), parts along dimension 0, may hold values from -3 to 0
- query: bfloat16 [12, 16, 128], P('gr', 'tp', 'sp'), parts along dimension 0, may hold values from -6 to 6
- out_gain: float32 [16, 128], P('tp'), may hold values from 0.1 to 1.9
Outputs:
- cache: bfloat16 [12, 16, 128, 128], P('gr', 'tp', 'sp'), parts along dimension 0
- read: float32 [12, 16, 128], P('gr', 'tp'), parts along dimension 0
There are 3 independent parts, one for each index of `gr`. A program takes and returns all parts, laid end to end along the dimension named above; an argument that names none is the same for every part. Nothing has to cross between parts.
All inputs are finite; a program needn't handle non-finite values.
Results may differ from a plain program's by a relative error of at most 0.0065.
Values sent between devices are 32-bit elements; how exact they have to be, the bound alone decides.
No kernel may reach another device: no remote copies, remote signals or barrier semaphores. Data moves between devices by JAX's collectives and lax.ppermute only.
A program may use at most 32 MiB of HBM per device.

v0:
```python
import jax
import jax.numpy as jnp
from jax import lax
from jax.sharding import PartitionSpec as P

epsilon = 1e-06


def from_everyone(value, axis):
    devices = lax.axis_size(axis)
    return lax.all_to_all(
        jnp.broadcast_to(value[None], (devices, *value.shape)), axis, 0, 0, tiled=True
    )


def taken_together(value, axis):
    everything = from_everyone(value, axis)
    return jnp.sum(everything, axis=0)


def normalize(row_block, gain_row):
    widened = row_block.astype(jnp.float32)
    scaled = widened * lax.rsqrt(jnp.mean(widened * widened, axis=-1, keepdims=True) + epsilon)
    return (scaled * gain_row).astype(jnp.bfloat16)


def settle(received):
    stacked, block_sums = received
    later_sum = jnp.cumsum(block_sums[::-1], axis=0)[::-1] - block_sums
    return jnp.sum(jnp.exp(later_sum)[..., None] * stacked, axis=0)


def local(tokens, new_tokens, in_gain, w_forget, w_value, gap, decay_shift, query, out_gain):
    seq_count, seg_len, model_width = tokens.shape
    head_count, key_dim = gap.shape
    val_dim = out_gain.shape[1]
    row_count = key_dim // lax.axis_size("sp")
    unit_norm_rows = normalize(tokens.reshape(seq_count * seg_len, model_width), in_gain)
    forget_pre = jnp.dot(unit_norm_rows, w_forget, preferred_element_type=jnp.float32).reshape(
        seq_count, seg_len, head_count, key_dim
    )
    values = jnp.dot(unit_norm_rows, w_value, preferred_element_type=jnp.float32).astype(
        jnp.bfloat16
    )
    values = values.reshape(seq_count, seg_len, head_count, val_dim)
    key_gate = gap * jax.nn.sigmoid(-forget_pre)
    forget_logarithm = jnp.log1p(-key_gate) + decay_shift[:, :, :, None]
    totals = jnp.sum(forget_logarithm, axis=1)
    within = totals[:, None] - jnp.cumsum(forget_logarithm, axis=1)
    weights = (key_gate * jnp.exp(within)).astype(jnp.bfloat16)
    pieces = jnp.einsum("sthi,sthj->shij", weights, values, preferred_element_type=jnp.float32)
    full_state = settle(
        (
            lax.all_to_all(pieces[None], "sp", split_axis=3, concat_axis=0, tiled=True),
            lax.all_to_all(totals[None], "sp", split_axis=3, concat_axis=0, tiled=True),
        )
    )
    cache = full_state.astype(jnp.bfloat16)
    row_start = lax.axis_index("sp") * row_count
    normed_new = normalize(new_tokens, in_gain)
    new_pre = jnp.dot(normed_new, w_forget, preferred_element_type=jnp.float32).reshape(
        seq_count, head_count, key_dim
    )
    new_key = lax.dynamic_slice_in_dim(gap * jax.nn.sigmoid(-new_pre), row_start, row_count, 2)
    new_values = lax.optimization_barrier(
        jnp.dot(normed_new, w_value, preferred_element_type=jnp.float32).astype(jnp.bfloat16)
    )
    new_values = new_values.astype(jnp.float32).reshape(seq_count, head_count, val_dim)
    updated = (1.0 - new_key)[..., None] * full_state + new_key[..., None] * new_values[
        :, :, None, :
    ]
    partial_value = jnp.einsum(
        "shi,shij->shj", query.astype(jnp.float32), updated, precision=lax.Precision.HIGHEST
    )
    read_raw = taken_together(partial_value, "sp")
    read = (
        read_raw
        * lax.rsqrt(jnp.mean(read_raw * read_raw, axis=-1, keepdims=True) + epsilon)
        * out_gain
    )
    return (cache, read)


def solution(mesh):
    return jax.shard_map(
        local,
        mesh=mesh,
        in_specs=(
            P("gr", "sp", None),
            P("gr", None),
            P(),
            P(None, "tp"),
            P(None, "tp"),
            P("tp", None),
            P("gr", "sp", "tp"),
            P("gr", "tp", "sp"),
            P("tp", None),
        ),
        out_specs=(P("gr", "tp", "sp", None), P("gr", "tp", None)),
        check_vma=False,
    )
```

profile of v0, /device:TPU:6, one launch (start us, length us, event | category | flops | bytes accessed | tf_op | source)
XLA Modules:
  0.0 86.7 jit_solution(9373078346931282527)
XLA Ops:
  0.7 4.3 %copy.85 = bf16[256,4096]{1,0:T(8,128)(2,1)} copy(bf16[256,4096]{0,1:T(8,128)(2,1)} %bitcast.63) | data formatting | bytes 4194304 | tf_op jit(solution)/shard_map/dot_general | solution.py:39
  4.9 4.2 %multiply_reduce_fusion = f32[4,192]{1,0:T(4,128)S(1)} fusion(bf16[4,192,4096]{2,1,0:T(8,128)(2,1)} %param.9), kind=kLoop, calls=%fused_computation.4 | loop fusion | flops 9436416 | bytes 6294528 | tf_op jit(solution)/shard_map/reduce_sum | solution.py:23
  9.2 0.3 copy-done.1
  9.5 4.0 %fusion.24 = (f32[4,128,2,192]{1,3,2,0:T(8,128)S(1)}, f32[4,192,2,128]{3,1,2,0:T(8,128)S(1)}) fusion(f32[4,2,192]{2,1,0:T(2,128)S(1)} %bitcast.71, f32[128,2]{0,1:T(2,128)S(1)} %bitcast.70, bf16[2,128,4096,1]{2,1,0,3:T(8,128)(2,1)} %bitcast.66, f32[4096]{0:T(1024)S(1)} %copy-done.3, f32[4,192]{1,0:T(4,128)S(1)} %add_rsqrt_fusion, ...), kind=kOutput, calls=%fused_computation.26 | convolution fusion | flops 1624178688 | bytes 9988096 | tf_op jit(solution)/shard_map/dot_general | solution.py:39
  13.5 0.9 %copy-done.2 = f32[4,192,2,128]{3,1,2,0:T(8,128)} copy-done((f32[4,192,2,128]{3,1,2,0:T(8,128)}, f32[4,192,2,128]{3,1,2,0:T(8,128)S(1)}, u32[]{:S(2)}) %copy-start.2) | copy-done | bytes 786456
  14.4 0.4 add_reduce_fusion
  14.8 0.8 copy.69
  15.6 13.0 %all-to-all-start = ((f32[1,4,2,128]{1,2,0,3:T(2,128)}), f32[1,4,2,128]{1,2,0,3:T(2,128)}, u32[]{:S(2)}, u32[]{:S(2)}) async-start(f32[1,4,2,128]{1,2,0,3:T(2,128)} %copy.69), calls=%async_computation | async-start | bytes 262144 | tf_op jit(solution)/shard_map/all_to_all | solution.py:55
  28.8 0.8 fusion.17
  29.7 0.4 broadcast_add_fusion
  30.1 0.1 copy.74
  30.2 5.3 %fusion.1 = bf16[768,4096]{1,0:T(8,128)(2,1)S(1)} fusion(f32[4096]{0:T(1024)S(1)} %copy-done.3, f32[768]{0:T(1024)S(1)} %rsqrt.29, bf16[4,192,4096]{2,1,0:T(8,128)(2,1)} %param.9), kind=kLoop, calls=%fused_computation.2 | loop fusion | flops 12582912 | bytes 12602368 | tf_op jit(solution)/shard_map/convert_element_type | solution.py:24
  35.5 2.6 %convolution_convert_fusion = bf16[768,256]{1,0:T(8,128)(2,1)} fusion(bf16[768,4096]{1,0:T(8,128)(2,1)S(1)} %fusion.1, bf16[4096,256]{1,0:T(8,128)(2,1)S(1)} %copy-done), kind=kOutput, calls=%fused_computation.9 | convolution fusion | flops 1610809344 | bytes 8781824 | tf_op jit(solution)/shard_map/dot_general | solution.py:42
  38.1 1.1 %reshape.85 = bf16[4,192,2,128]{3,2,1,0:T(2,128)(2,1)S(1)} reshape(bf16[768,256]{1,0:T(8,128)(2,1)} %convolution_convert_fusion) | data formatting | bytes 786432 | tf_op jit(solution)/shard_map/reshape | solution.py:45
  39.2 1.5 %convolution_bitcast_fusion = f32[1,4,2,128,128]{4,3,2,1,0:T(8,128)S(1)} fusion(f32[4,256,2,128]{3,1,2,0:T(8,128)S(1)} %bitcast.65, f32[4,192,2,128]{3,1,2,0:T(8,128)} %copy-done.2, bf16[4,192,2,128]{3,2,1,0:T(2,128)(2,1)S(1)} %reshape.85, f32[4,2,128]{2,1,0:T(2,128)} %copy-done.4, f32[2,128]{1,0:T(2,128)} %param.14), kind=kOutput, calls=%fused_computation.10 | convolution fusion | flops 51118080 | bytes 2495488 | tf_op jit(solution)/shard_map/sthi,sthj->shij/dot_general | solution.py:51
  40.7 1.2 %copy.76 = f32[1,4,2,128,128]{4,2,1,0,3:T(2,128)} copy(f32[1,4,2,128,128]{4,3,2,1,0:T(8,128)S(1)} %convolution_bitcast_fusion) | data formatting | bytes 1048576 | tf_op jit(solution)/shard_map/broadcast_in_dim | solution.py:54
  41.9 10.1 %all-to-all-start.1 = ((f32[1,4,2,128,128]{4,2,1,0,3:T(2,128)}), f32[1,4,2,128,128]{4,2,1,0,3:T(2,128)S(1)}, u32[]{:S(2)}, u32[]{:S(2)}) async-start(f32[1,4,2,128,128]{4,2,1,0,3:T(2,128)} %copy.76), calls=%async_computation.1 | async-start | bytes 1048576 | tf_op jit(solution)/shard_map/all_to_all | solution.py:54
  52.0 0.9 %fusion.29 = f32[4]{0:T(128)S(1)} fusion(bf16[4,4096]{1,0:T(4,128)(2,1)} %param.10), kind=kLoop, calls=%fused_computation.36 | loop fusion | flops 49148 | bytes 32784 | tf_op jit(solution)/shard_map/reduce_sum | solution.py:23
  52.9 1.2 %convolution_convert_fusion.1 = bf16[4,256]{1,0:T(4,128)(2,1)S(1)} fusion(bf16[4096,256]{1,0:T(8,128)(2,1)S(1)} %copy-done, bf16[4,4096]{1,0:T(4,128)(2,1)} %param.10, f32[4096]{0:T(1024)S(1)} %copy-done.3, f32[4]{0:T(128)S(1)} %add_rsqrt_fusion.2), kind=kOutput, calls=%fused_computation.15 | convolution fusion | flops 8455168 | bytes 2148368 | tf_op jit(solution)/shard_map/dot_general | solution.py:66
  54.1 0.8 constant_dynamic-slice_fusion
  54.9 2.0 %fusion.13 = f32[4,2,128]{2,0,1:T(4,128)S(1)} fusion(bf16[4096,256]{1,0:T(8,128)(2,1)} %param.12, bf16[4,4096]{1,0:T(4,128)(2,1)} %param.10, f32[4096]{0:T(1024)S(1)} %copy-done.3, f32[4]{0:T(128)S(1)} %add_rsqrt_fusion.2), kind=kOutput, calls=%fused_computation.14 | convolution fusion | flops 8456192 | bytes 2150416 | tf_op jit(solution)/shard_map/dot_general | solution.py:61
  57.0 0.1 copy.78
  57.2 1.4 %copy.71 = f32[1,4,2,32,4]{4,2,1,3,0:T(2,128)S(1)} copy(f32[1,4,2,32,4]{1,2,4,3,0:T(2,128)} %bitcast.6) | data formatting | bytes 8192 | tf_op jit(solution)/shard_map/all_to_all | solution.py:55
  58.8 0.9 %copy.72 = f32[32,4,2,4]{2,1,3,0:T(4,128)S(1)} copy(f32[32,4,2,4]{3,2,1,0:T(2,128)S(1)} %subtract_exponential_fusion) | data formatting | bytes 8192 | tf_op jit(solution)/shard_map/exp | solution.py:30
  59.7 8.7 %all-to-all-done.1 = f32[1,4,2,128,128]{4,2,1,0,3:T(2,128)S(1)} async-done(((f32[1,4,2,128,128]{4,2,1,0,3:T(2,128)}), f32[1,4,2,128,128]{4,2,1,0,3:T(2,128)S(1)}, u32[]{:S(2)}, u32[]{:S(2)}) %all-to-all-start.1) | async-done | bytes 524320 | tf_op jit(solution)/shard_map/all_to_all | solution.py:54
  68.4 0.7 multiply_reduce_fusion.1
  69.2 0.2 fusion.32
  69.3 0.7 broadcast_in_dim.8
  70.0 5.3 %all-to-all-start.2 = ((f32[32,4,2,128]{3,2,1,0:T(2,128)}), f32[32,4,2,128]{3,2,1,0:T(2,128)S(1)}, u32[]{:S(2)}, u32[]{:S(2)}) async-start(f32[32,4,2,128]{3,2,1,0:T(2,128)} %broadcast_in_dim.8), calls=%async_computation.2 | async-start | bytes 262144 | tf_op jit(solution)/shard_map/all_to_all | solution.py:11
  75.3 0.6 copy.80
  75.9 9.9 %all-to-all-done.2 = f32[32,4,2,128]{3,2,1,0:T(2,128)S(1)} async-done(((f32[32,4,2,128]{3,2,1,0:T(2,128)}), f32[32,4,2,128]{3,2,1,0:T(2,128)S(1)}, u32[]{:S(2)}, u32[]{:S(2)}) %all-to-all-start.2) | async-done | bytes 131104 | tf_op jit(solution)/shard_map/all_to_all | solution.py:11
  86.0 0.7 multiply_multiply_fusion
  (34 shorter events, 0.9 us)
Async XLA Ops:
  0.6 34.9 %copy-start = (bf16[4096,256]{1,0:T(8,128)(2,1)S(1)}, bf16[4096,256]{1,0:T(8,128)(2,1)}, u32[]{:S(2)}) copy-start(bf16[4096,256]{1,0:T(8,128)(2,1)} %param.13) | copy-start | bytes 6291460
  0.6 8.6 %copy-start.6 = (f32[4,192,2]{1,2,0:T(2,128)S(1)}, f32[4,192,2]{1,2,0:T(2,128)}, u32[]{:S(2)}) copy-start(f32[4,192,2]{1,2,0:T(2,128)} %param.15) | copy-start | bytes 18436
  0.7 8.6 %copy-start.5 = (f32[2,128]{1,0:T(2,128)S(1)}, f32[2,128]{1,0:T(2,128)}, u32[]{:S(2)}) copy-start(f32[2,128]{1,0:T(2,128)} %param.14) | copy-start | bytes 3076
  0.7 8.5 %copy-start.3 = (f32[4096]{0:T(1024)S(1)}, f32[4096]{0:T(1024)}, u32[]{:S(2)}) copy-start(f32[4096]{0:T(1024)} %param.11) | copy-start | bytes 49156
  4.9 4.6 %copy-start.1 = (bf16[4,192,4096]{2,1,0:T(8,128)(2,1)S(1)}, bf16[4,192,4096]{2,1,0:T(8,128)(2,1)}, u32[]{:S(2)}) copy-start(bf16[4,192,4096]{2,1,0:T(8,128)(2,1)} %param.9) | copy-start | bytes 18874372
  13.5 0.9 %copy-start.2 = (f32[4,192,2,128]{3,1,2,0:T(8,128)}, f32[4,192,2,128]{3,1,2,0:T(8,128)S(1)}, u32[]{:S(2)}) copy-start(f32[4,192,2,128]{3,1,2,0:T(8,128)S(1)} %get-tuple-element.15) | copy-start | bytes 2359300
  14.8 14.0 %copy-start.4 = (f32[4,2,128]{2,1,0:T(2,128)}, f32[4,2,128]{2,1,0:T(2,128)S(1)}, u32[]{:S(2)}) copy-start(f32[4,2,128]{2,1,0:T(2,128)S(1)} %add_reduce_fusion) | copy-start | bytes 12292
  15.6 26.4 %all-to-all-start = ((f32[1,4,2,128]{1,2,0,3:T(2,128)}), f32[1,4,2,128]{1,2,0,3:T(2,128)}, u32[]{:S(2)}, u32[]{:S(2)}) async-start(f32[1,4,2,128]{1,2,0,3:T(2,128)} %copy.69), calls=%async_computation | async-start | bytes 262144 | tf_op jit(solution)/shard_map/all_to_all | solution.py:55
  40.7 28.4 %copy-start.8 = (bf16[4,2,4]{2,1,0:T(2,128)(2,1)S(1)}, bf16[4,2,4]{2,1,0:T(2,128)(2,1)}, u32[]{:S(2)}) copy-start(bf16[4,2,4]{2,1,0:T(2,128)(2,1)} %param.16) | copy-start | bytes 196
  40.7 45.2 %copy-start.7 = (f32[2,128]{1,0:T(2,128)S(1)}, f32[2,128]{1,0:T(2,128)}, u32[]{:S(2)}) copy-start(f32[2,128]{1,0:T(2,128)} %param.17) | copy-start | bytes 3076
  41.9 26.4 %all-to-all-start.1 = ((f32[1,4,2,128,128]{4,2,1,0,3:T(2,128)}), f32[1,4,2,128,128]{4,2,1,0,3:T(2,128)S(1)}, u32[]{:S(2)}, u32[]{:S(2)}) async-start(f32[1,4,2,128,128]{4,2,1,0,3:T(2,128)} %copy.76), calls=%async_computation.1 | async-start | bytes 1048576 | tf_op jit(solution)/shard_map/all_to_all | solution.py:54
  70.0 15.8 %all-to-all-start.2 = ((f32[32,4,2,128]{3,2,1,0:T(2,128)}), f32[32,4,2,128]{3,2,1,0:T(2,128)S(1)}, u32[]{:S(2)}, u32[]{:S(2)}) async-start(f32[32,4,2,128]{3,2,1,0:T(2,128)} %broadcast_in_dim.8), calls=%async_computation.2 | async-start | bytes 262144 | tf_op jit(solution)/shard_map/all_to_all | solution.py:11
where the time goes:
time: 87.4 us; the launch traced here: 86.7 us
  starting transfers between devices  28.4 us (32%)
  waiting for transfers between devices  18.6 us (21%)
  other arithmetic  13.9 us (16%)
  local copies, waits for them, and re-layouts  13.4 us (15%)
  matrix products  11.4 us (13%)
  between operations  0.88 us (1%)
    all_to_all x1, starting transfers between devices, local(): lax.all_to_all(totals[None], 'sp', split_axis=3, concat_axis=0, tiled=True)  13 us
    all_to_all x1, starting transfers between devices, local(): lax.all_to_all(pieces[None], 'sp', split_axis=3, concat_axis=0, tiled=True)  10.1 us
    all_to_all x1, waiting for transfers between devices, from_everyone(): lax.all_to_all(jnp.broadcast_to(value[None], (devices, *value.shape)), ax...  9.9 us
    all_to_all x1, waiting for transfers between devices, local(): lax.all_to_all(pieces[None], 'sp', split_axis=3, concat_axis=0, tiled=True)  8.69 us
    convert_element_type x1, other arithmetic, normalize(): return (scaled * gain_row).astype(jnp.bfloat16)  5.33 us
    all_to_all x1, starting transfers between devices, from_everyone(): lax.all_to_all(jnp.broadcast_to(value[None], (devices, *value.shape)), ax...  5.3 us
    reduce_sum x2, other arithmetic, normalize(): jnp.mean(widened * widened, axis=-1, keepdims=True) + epsilon  5.14 us
    dot_general x1, local copies, waits for them, and re-layouts, local(): jnp.dot(unit_norm_rows, w_forget, preferred_element_type=jnp.float32)  4.27 us
  transfers between devices with their start and end apart: 3, of which 2 were waited for; matrix products, arithmetic and copies ran while one was open for 25% of the time, Pallas kernels for 0%

commit v1 on v0

v1 whole, which is shorter than its diff:
```python
import functools

import jax
import jax.numpy as jnp
from jax import lax
from jax.experimental import pallas as pl
from jax.experimental.pallas import tpu as pltpu
from jax.sharding import PartitionSpec as P

epsilon = 1e-06

STATE_ROWS = 32
BLOCK_ROWS = 33
K_BLOCK = 512


def segment_kernel(
    seqs, heads, key_dim, steps,
    tok_ref, new_ref, gain_ref, wf_ref, wv_ref, gap_ref, shift_ref,
    buf_ref, nk_ref, nv_ref,
    accf, accv, ssq, pieces, shift_cols, total_cols,
):
    step = pl.program_id(0)
    seg = tok_ref.shape[1]
    rows = seqs * seg
    width = heads * key_dim
    pad = accf.shape[0] - rows
    groups = seqs * heads
    rank = BLOCK_ROWS
    per = STATE_ROWS // groups
    devices = key_dim // per

    tok = tok_ref[...].reshape(rows, tok_ref.shape[2])
    new = new_ref[...].astype(jnp.float32)
    new = jnp.concatenate([new, jnp.zeros((pad - seqs, new.shape[1]), jnp.float32)], axis=0)
    wide = jnp.concatenate([tok.astype(jnp.float32), new], axis=0)
    squares = wide * wide
    part = squares[:, 0:128]
    for c in range(1, squares.shape[1] // 128):
        part = part + squares[:, c * 128 : (c + 1) * 128]
    x = (wide * gain_ref[...]).astype(jnp.bfloat16)
    yf = jnp.dot(x, wf_ref[...], preferred_element_type=jnp.float32)
    yv = jnp.dot(x, wv_ref[...], preferred_element_type=jnp.float32)

    @pl.when(step == 0)
    def _():
        accf[...] = yf
        accv[...] = yv
        ssq[...] = part
        shift_rows = jnp.concatenate(
            [shift_ref[s] for s in range(seqs)]
            + [jnp.zeros((128 - groups, seg), jnp.float32)], axis=0)
        shift_rows = jnp.concatenate(
            [shift_rows, jnp.zeros((128, 256 - seg), jnp.float32)], axis=1)
        shift_cols[...] = shift_rows.T

    @pl.when(step > 0)
    def _():
        accf[...] += yf
        accv[...] += yv
        ssq[...] += part

    @pl.when(step == steps - 1)
    def _():
        model_width = steps * tok_ref.shape[2]
        gap_row = jnp.concatenate([gap_ref[h : h + 1, :] for h in range(heads)], axis=1)
        ti = lax.broadcasted_iota(jnp.int32, (seg, seg), 0)
        tj = lax.broadcasted_iota(jnp.int32, (seg, seg), 1)
        later = (tj > ti).astype(jnp.float32).astype(jnp.bfloat16)
        total_rows = []
        for s in range(seqs):
            here = slice(s * seg, (s + 1) * seg)
            scale = lax.rsqrt(
                jnp.sum(ssq[here, :], axis=1, keepdims=True) / model_width + epsilon)
            key_gate = gap_row * jax.nn.sigmoid(-(accf[here, :] * scale))
            shift = jnp.concatenate(
                [jnp.broadcast_to(shift_cols[0:seg, s * heads + h : s * heads + h + 1],
                                  (seg, key_dim)) for h in range(heads)], axis=1)
            log_forget = jnp.log1p(-key_gate) + shift
            high = log_forget.astype(jnp.bfloat16)
            low = (log_forget - high.astype(jnp.float32)).astype(jnp.bfloat16)
            within = jnp.dot(later, high, preferred_element_type=jnp.float32)
            within = within + jnp.dot(later, low, preferred_element_type=jnp.float32)
            weights = (key_gate * jnp.exp(within)).astype(jnp.bfloat16)
            values = (accv[here, :] * scale).astype(jnp.bfloat16)
            total = jnp.sum(log_forget, axis=0, keepdims=True)
            for h in range(heads):
                lanes = slice(h * key_dim, (h + 1) * key_dim)
                group = s * heads + h
                total_rows.append(total[:, lanes])
                pieces[...] = lax.dot_general(
                    weights[:, lanes], values[:, lanes], (((0,), (0,)), ((), ())),
                    preferred_element_type=jnp.float32)
                for i in range(per):
                    buf_ref[pl.ds(i * groups + group, devices, stride=rank), :] = (
                        pieces[pl.ds(i, devices, stride=per), :])
        totals = jnp.concatenate(
            total_rows + [jnp.zeros((128 - groups, key_dim), jnp.float32)], axis=0)
        total_cols[...] = totals.T
        packed = total_cols[pl.ds(0, devices, stride=per), :]
        for i in range(1, per):
            packed = packed + pltpu.roll(
                total_cols[pl.ds(i, devices, stride=per), :], i * groups, 1)
        buf_ref[pl.ds(STATE_ROWS, devices, stride=rank), :] = packed
        for extra in range(STATE_ROWS + 1, rank):
            buf_ref[pl.ds(extra, devices, stride=rank), :] = jnp.zeros_like(packed)

        last = slice(rows, rows + pad)
        scale = lax.rsqrt(
            jnp.sum(ssq[last, :], axis=1, keepdims=True) / model_width + epsilon)
        new_key = gap_row * jax.nn.sigmoid(-(accf[last, :] * scale))
        new_values = (accv[last, :] * scale).astype(jnp.bfloat16).astype(jnp.float32)
        for h in range(heads):
            lanes = slice(h * key_dim, (h + 1) * key_dim)
            nk_ref[pl.ds(h, seqs, stride=heads), :] = new_key[0:seqs, lanes]
            nv_ref[pl.ds(h, seqs, stride=heads), :] = new_values[0:seqs, lanes]


def settle_kernel(
    devices, per,
    place_ref, got_ref, nk_ref, nv_ref, query_ref,
    state_ref, part_ref,
):
    groups = nk_ref.shape[0]
    totals = got_ref[pl.ds(STATE_ROWS, devices, stride=BLOCK_ROWS), :]
    cols = jnp.concatenate(
        [totals, jnp.zeros((128 - devices, 128), jnp.float32)], axis=0).T[0:STATE_ROWS]
    later = pltpu.roll(cols, 127, 1)
    reach = 1
    while reach < devices:
        later = later + pltpu.roll(later, 128 - reach, 1)
        reach *= 2
    factor = jnp.exp(later)
    lane = lax.broadcasted_iota(jnp.int32, (groups, 128), 1)
    first = place_ref[0] * per
    query = jnp.concatenate(
        [query_ref[s].astype(jnp.float32) for s in range(query_ref.shape[0])], axis=0)
    part = jnp.zeros((groups, 128), jnp.float32)
    for i in range(per):
        base = i * groups
        state = factor[base : base + groups, 0:1] * got_ref[base : base + groups, :]
        for g in range(1, devices):
            start = g * BLOCK_ROWS + base
            state = state + factor[base : base + groups, g : g + 1] * got_ref[
                start : start + groups, :]
        state_ref[pl.ds(i, groups, stride=per), :] = state
        new_key = jnp.sum(
            jnp.where(lane == first + i, nk_ref[...], 0.0), axis=1, keepdims=True)
        updated = (1.0 - new_key) * state + new_key * nv_ref[...]
        part = part + query[:, i : i + 1] * updated
    for d in range(devices):
        part_ref[d * groups : (d + 1) * groups, :] = part


def read_kernel(devices, got_ref, gain_ref, read_ref):
    seqs, heads, val_dim = read_ref.shape
    groups = seqs * heads
    raw = got_ref[0:groups, :]
    for d in range(1, devices):
        raw = raw + got_ref[d * groups : (d + 1) * groups, :]
    gain = jnp.concatenate([gain_ref[...]] * seqs, axis=0)
    mean = jnp.sum(raw * raw, axis=1, keepdims=True) / val_dim
    out = raw * lax.rsqrt(mean + epsilon) * gain
    for s in range(seqs):
        read_ref[s] = out[s * heads : (s + 1) * heads, :]


def local(tokens, new_tokens, in_gain, w_forget, w_value, gap, decay_shift, query, out_gain):
    seqs, seg, model_width = tokens.shape
    heads, key_dim = gap.shape
    val_dim = out_gain.shape[1]
    width = heads * key_dim
    devices = lax.axis_size("sp")
    per = key_dim // devices
    groups = seqs * heads
    steps = model_width // K_BLOCK
    rows = seqs * seg + 16
    whole = pl.BlockSpec(memory_space=pltpu.VMEM)
    f32 = jnp.float32
    buf, new_key, new_values = pl.pallas_call(
        functools.partial(segment_kernel, seqs, heads, key_dim, steps),
        grid=(steps,),
        in_specs=[
            pl.BlockSpec((seqs, seg, K_BLOCK), lambda k: (0, 0, k)),
            pl.BlockSpec((seqs, K_BLOCK), lambda k: (0, k)),
            pl.BlockSpec((1, K_BLOCK), lambda k: (0, k)),
            pl.BlockSpec((K_BLOCK, width), lambda k: (k, 0)),
            pl.BlockSpec((K_BLOCK, width), lambda k: (k, 0)),
            pl.BlockSpec((heads, key_dim), lambda k: (0, 0)),
            pl.BlockSpec((seqs, heads, seg), lambda k: (0, 0, 0)),
        ],
        out_specs=[
            pl.BlockSpec((devices * BLOCK_ROWS, val_dim), lambda k: (0, 0)),
            pl.BlockSpec((groups, key_dim), lambda k: (0, 0)),
            pl.BlockSpec((groups, val_dim), lambda k: (0, 0)),
        ],
        out_shape=[
            jax.ShapeDtypeStruct((devices * BLOCK_ROWS, val_dim), f32),
            jax.ShapeDtypeStruct((groups, key_dim), f32),
            jax.ShapeDtypeStruct((groups, val_dim), f32),
        ],
        scratch_shapes=[
            pltpu.VMEM((rows, width), f32),
            pltpu.VMEM((rows, width), f32),
            pltpu.VMEM((rows, 128), f32),
            pltpu.VMEM((key_dim, val_dim), f32),
            pltpu.VMEM((256, 128), f32),
            pltpu.VMEM((128, 128), f32),
        ],
        compiler_params=pltpu.CompilerParams(
            dimension_semantics=("arbitrary",)),
        name="segment",
    )(
        tokens, new_tokens, in_gain.reshape(1, model_width), w_forget, w_value, gap,
        jnp.transpose(decay_shift, (0, 2, 1)),
    )
    got = lax.all_to_all(
        buf.reshape(devices, BLOCK_ROWS, 1, val_dim), "sp", 0, 0, tiled=True
    ).reshape(devices * BLOCK_ROWS, val_dim)
    place = lax.axis_index("sp").astype(jnp.int32).reshape(1)
    state, part = pl.pallas_call(
        functools.partial(settle_kernel, devices, per),
        in_specs=[pl.BlockSpec(memory_space=pltpu.SMEM), whole, whole, whole, whole],
        out_specs=[whole, whole],
        out_shape=[
            jax.ShapeDtypeStruct((STATE_ROWS, val_dim), f32),
            jax.ShapeDtypeStruct((devices * groups, val_dim), f32),
        ],
        compiler_params=pltpu.CompilerParams(vmem_limit_bytes=8 * 2**20),
        name="settle",
    )(place, got, new_key, new_values, query)
    everything = lax.all_to_all(
        part.reshape(devices, groups, val_dim), "sp", 0, 0, tiled=True
    ).reshape(devices * groups, val_dim)
    cache = state.astype(jnp.bfloat16).reshape(seqs, heads, per, val_dim)
    read = pl.pallas_call(
        functools.partial(read_kernel, devices),
        in_specs=[whole, whole],
        out_specs=whole,
        out_shape=jax.ShapeDtypeStruct((seqs, heads, val_dim), f32),
        compiler_params=pltpu.CompilerParams(vmem_limit_bytes=8 * 2**20),
        name="read",
    )(everything, out_gain)
    return (cache, read)


def solution(mesh):
    return jax.shard_map(
        local,
        mesh=mesh,
        in_specs=(
            P("gr", "sp", None),
            P("gr", None),
            P(),
            P(None, "tp"),
            P(None, "tp"),
            P("tp", None),
            P("gr", "sp", "tp"),
            P("gr", "tp", "sp"),
            P("tp", None),
        ),
        out_specs=(P("gr", "tp", "sp", None), P("gr", "tp", None)),
        check_vma=False,
    )
```

time: 87.4 us -> 62.8 us (0.72)
  Pallas kernels: 0 us -> 14.4 us
  other arithmetic: 13.9 us -> 0.6 us
  local copies, waits for them, and re-layouts: 13.4 us -> 1.38 us
  matrix products: 11.4 us -> 0 us
  starting transfers between devices: 28.4 us -> 18.4 us
  waiting for transfers between devices: 18.6 us -> 26.9 us
    pallas_call x0 -> x3, Pallas kernels: none -> 14.4 us  [the longest x1 12.3 us: local(): pl.pallas_call(functools.partial(segment_kernel, seqs, heads, key_dim, st...]
    dot_general x6 -> x0, matrix products: 11.4 us -> none  [the longest x1 3.99 us: local(): jnp.dot(unit_norm_rows, w_forget, preferred_element_type=jnp.float32)]
    all_to_all x3 -> x2, starting transfers between devices: 28.4 us -> 18.4 us  [the longest x1 12.9 us: local(): lax.all_to_all(buf.reshape(devices, BLOCK_ROWS, 1, val_dim), 'sp', 0, 0,...]
    all_to_all x3 -> x2, waiting for transfers between devices: 18.6 us -> 26.9 us  [the longest x1 17 us: local(): lax.all_to_all(buf.reshape(devices, BLOCK_ROWS, 1, val_dim), 'sp', 0, 0,...]
    reduce_sum x6 -> x0, other arithmetic: 6.35 us -> none  [the longest x2 5.14 us: normalize(): jnp.mean(widened * widened, axis=-1, keepdims=True) + epsilon]
    convert_element_type x1, other arithmetic: 5.33 us -> 0.6 us  [local(): cache = state.astype(jnp.bfloat16).reshape(seqs, heads, per, val_dim)]
    dot_general x1 -> x0, local copies, waits for them, and re-layouts: 4.27 us -> none  [local(): jnp.dot(unit_norm_rows, w_forget, preferred_element_type=jnp.float32)]
    broadcast_in_dim x3 -> x0, local copies, waits for them, and re-layouts: 2.67 us -> none  [the longest x1 1.19 us: local(): pieces[None]]
  transfers between devices with their start and end apart: 3 -> 2, of which waited for: 2 -> 2; matrix products, arithmetic and copies ran while one was open for 25% -> 1% of each run, Pallas kernels for 0% -> 0%
where the time goes in v1:
time: 62.8 us; the launch traced here: 62.4 us
  waiting for transfers between devices  26.9 us (43%)
  starting transfers between devices  18.4 us (29%)
  Pallas kernels  14.4 us (23%)
  local copies, waits for them, and re-layouts  1.38 us (2%)
  between operations  0.67 us (1%)
    all_to_all x1, waiting for transfers between devices, local(): lax.all_to_all(buf.reshape(devices, BLOCK_ROWS, 1, val_dim), 'sp', 0, 0,...  17 us
    all_to_all x1, starting transfers between devices, local(): lax.all_to_all(buf.reshape(devices, BLOCK_ROWS, 1, val_dim), 'sp', 0, 0,...  12.9 us
    pallas_call x1, Pallas kernels, local(): pl.pallas_call(functools.partial(segment_kernel, seqs, heads, key_dim, st...  12.3 us
    all_to_all x1, waiting for transfers between devices, local(): lax.all_to_all(part.reshape(devices, groups, val_dim), 'sp', 0, 0, tiled=...  9.89 us
    all_to_all x1, starting transfers between devices, local(): lax.all_to_all(part.reshape(devices, groups, val_dim), 'sp', 0, 0, tiled=...  5.49 us
    pallas_call x1, Pallas kernels, local(): pl.pallas_call(functools.partial(settle_kernel, devices, per), in_specs=[...  1.42 us
    unnamed x8, local copies, waits for them, and re-layouts  1.38 us
  transfers between devices with their start and end apart: 2, of which 2 were waited for; matrix products, arithmetic and copies ran while one was open for 1% of the time, Pallas kernels for 0%

profile of v1, /device:TPU:6, one launch (start us, length us, event | category | flops | bytes accessed | tf_op | source)
XLA Modules:
  0.0 62.4 jit_solution(10156793831543072609)
XLA Ops:
  0.6 0.0 copy-start.2
  0.6 0.0 copy-start.3
  0.7 12.3 %segment.1 = (f32[1056,128]{1,0:T(8,128)}, f32[8,128]{1,0:T(8,128)}, f32[8,128]{1,0:T(8,128)}) custom-call(bf16[4,192,4096]{2,1,0:T(8,128)(2,1)} %tok_ref.1, bf16[4,4096]{1,0:T(4,128)(2,1)} %new_ref.1, f32[1,4096]{1,0:T(1,128)} %bitcast.11, bf16[4096,256]{1,0:T(8,128)(2,1)} %wf_ref.1, bf16[4096,256]{1,0:T(8,128)(2,1)} %wv_ref.1, f32[2,128]{1,0:T(2,128)} %gap_ref.1, ...), custom_call_target="tpu_custom_call" | custom-call | tf_op jit(solution)/shard_map/segment/pallas_call | solution.py:180
  12.9 12.9 %all-to-all-start = ((f32[32,33,1,128]{3,2,1,0:T(1,128)}), f32[32,33,1,128]{3,2,1,0:T(1,128)S(1)}, u32[]{:S(2)}, u32[]{:S(2)}) async-start(f32[32,33,1,128]{3,2,1,0:T(1,128)} %bitcast.10), calls=%async_computation | async-start | bytes 1081344 | tf_op jit(solution)/shard_map/all_to_all | solution.py:217
  25.9 17.0 %all-to-all-done = f32[32,33,1,128]{3,2,1,0:T(1,128)S(1)} async-done(((f32[32,33,1,128]{3,2,1,0:T(1,128)}), f32[32,33,1,128]{3,2,1,0:T(1,128)S(1)}, u32[]{:S(2)}, u32[]{:S(2)}) %all-to-all-start) | async-done | bytes 540704 | tf_op jit(solution)/shard_map/all_to_all | solution.py:217
  42.8 0.0 copy-done.2
  42.8 0.0 copy-start
  42.8 0.7 %copy-done = f32[8,128]{1,0:T(8,128)S(1)} copy-done((f32[8,128]{1,0:T(8,128)S(1)}, f32[8,128]{1,0:T(8,128)}, u32[]{:S(2)}) %copy-start) | copy-done | bytes 4120
  43.5 0.0 copy-start.1
  43.5 0.7 %copy-done.1 = f32[8,128]{1,0:T(8,128)S(1)} copy-done((f32[8,128]{1,0:T(8,128)S(1)}, f32[8,128]{1,0:T(8,128)}, u32[]{:S(2)}) %copy-start.1) | copy-done | bytes 4120
  44.2 1.4 %settle.1 = (f32[32,128]{1,0:T(8,128)S(1)}, f32[256,128]{1,0:T(8,128)}) custom-call(s32[1]{0:T(128)} %bitcast.place_ref, f32[1056,128]{1,0:T(8,128)S(1)} %bitcast.8, f32[8,128]{1,0:T(8,128)S(1)} %copy-done, f32[8,128]{1,0:T(8,128)S(1)} %copy-done.1, bf16[4,2,4]{2,1,0:T(2,128)(2,1)S(1)} %copy-done.2), custom_call_target="tpu_custom_call" | custom-call | tf_op jit(solution)/shard_map/settle/pallas_call | solution.py:221
  45.6 5.5 %all-to-all-start.1 = ((f32[32,8,128]{2,1,0:T(8,128)}), f32[32,8,128]{2,1,0:T(8,128)S(1)}, u32[]{:S(2)}, u32[]{:S(2)}) async-start(f32[32,8,128]{2,1,0:T(8,128)} %bitcast.6), calls=%async_computation.1 | async-start | bytes 262144 | tf_op jit(solution)/shard_map/all_to_all | solution.py:232
  51.1 0.6 convert_element_type.3
  51.7 9.9 %all-to-all-done.1 = f32[32,8,128]{2,1,0:T(8,128)S(1)} async-done(((f32[32,8,128]{2,1,0:T(8,128)}), f32[32,8,128]{2,1,0:T(8,128)S(1)}, u32[]{:S(2)}, u32[]{:S(2)}) %all-to-all-start.1) | async-done | bytes 131104 | tf_op jit(solution)/shard_map/all_to_all | solution.py:232
  61.6 0.0 copy-done.3
  61.6 0.7 %read.1 = f32[4,2,128]{2,1,0:T(2,128)} custom-call(f32[256,128]{1,0:T(8,128)S(1)} %bitcast.9, f32[2,128]{1,0:T(2,128)S(1)} %copy-done.3), custom_call_target="tpu_custom_call" | custom-call | tf_op jit(solution)/shard_map/read/pallas_call | solution.py:236
Async XLA Ops:
  0.6 42.2 %copy-start.2 = (bf16[4,2,4]{2,1,0:T(2,128)(2,1)S(1)}, bf16[4,2,4]{2,1,0:T(2,128)(2,1)}, u32[]{:S(2)}) copy-start(bf16[4,2,4]{2,1,0:T(2,128)(2,1)} %query_ref.1) | copy-start | bytes 196
  0.6 61.0 %copy-start.3 = (f32[2,128]{1,0:T(2,128)S(1)}, f32[2,128]{1,0:T(2,128)}, u32[]{:S(2)}) copy-start(f32[2,128]{1,0:T(2,128)} %gain_ref.1) | copy-start | bytes 3076
  12.9 29.9 %all-to-all-start = ((f32[32,33,1,128]{3,2,1,0:T(1,128)}), f32[32,33,1,128]{3,2,1,0:T(1,128)S(1)}, u32[]{:S(2)}, u32[]{:S(2)}) async-start(f32[32,33,1,128]{3,2,1,0:T(1,128)} %bitcast.10), calls=%async_computation | async-start | bytes 1081344 | tf_op jit(solution)/shard_map/all_to_all | solution.py:217
  42.8 0.7 %copy-start = (f32[8,128]{1,0:T(8,128)S(1)}, f32[8,128]{1,0:T(8,128)}, u32[]{:S(2)}) copy-start(f32[8,128]{1,0:T(8,128)} %get-tuple-element.8.nk_ref) | copy-start | bytes 12292
  43.5 0.7 %copy-start.1 = (f32[8,128]{1,0:T(8,128)S(1)}, f32[8,128]{1,0:T(8,128)}, u32[]{:S(2)}) copy-start(f32[8,128]{1,0:T(8,128)} %get-tuple-element.9.nv_ref) | copy-start | bytes 12292
  45.6 16.0 %all-to-all-start.1 = ((f32[32,8,128]{2,1,0:T(8,128)}), f32[32,8,128]{2,1,0:T(8,128)S(1)}, u32[]{:S(2)}, u32[]{:S(2)}) async-start(f32[32,8,128]{2,1,0:T(8,128)} %bitcast.6), calls=%async_computation.1 | async-start | bytes 262144 | tf_op jit(solution)/shard_map/all_to_all | solution.py:232

commit v2 on v1

v2 whole, which is shorter than its diff:
```python
import functools

import jax
import jax.numpy as jnp
from jax import lax
from jax.experimental import pallas as pl
from jax.experimental.pallas import tpu as pltpu
from jax.sharding import PartitionSpec as P

epsilon = 1e-06

STATE_ROWS = 32
BLOCK_ROWS = 33
CHUNKS = (512, 512, 1024, 1024, 1024)
VMEM_MIB = 48


def segment_kernel(
    seqs, heads, key_dim, chunks,
    tok_hbm, new_hbm, gain_hbm, wf_hbm, wv_hbm, gap_hbm, shift_hbm,
    buf_ref, nk_ref, nv_ref,
    tok_ref, wf_ref, wv_ref, new_ref, gain_ref, gap_ref, shift_ref, accf, accv, ssq, pieces, shift_cols, total_cols, sems,
):
    seg = tok_ref.shape[1]
    model_width = tok_ref.shape[2]
    rows = seqs * seg
    pad = accf.shape[0] - rows
    groups = seqs * heads
    rank = BLOCK_ROWS
    per = STATE_ROWS // groups
    devices = key_dim // per

    small = [
        pltpu.make_async_copy(source, target, sems.at[3, n])
        for n, (source, target) in enumerate(
            ((new_hbm, new_ref), (gain_hbm, gain_ref), (gap_hbm, gap_ref),
             (shift_hbm, shift_ref)))
    ]
    copies = []
    start = 0
    for n, size in enumerate(chunks):
        cols = slice(start, start + size)
        trio = [
            pltpu.make_async_copy(wf_hbm.at[cols, :], wf_ref.at[cols, :], sems.at[0, n]),
            pltpu.make_async_copy(wv_hbm.at[cols, :], wv_ref.at[cols, :], sems.at[1, n]),
            pltpu.make_async_copy(tok_hbm.at[:, :, cols], tok_ref.at[:, :, cols], sems.at[2, n]),
        ]
        for copy in trio:
            copy.start()
        if n == 0:
            for copy in small:
                copy.start()
        copies.append((cols, trio))
        start += size
    for copy in small:
        copy.wait()
    shift_rows = jnp.concatenate(
        [shift_ref[s] for s in range(seqs)]
        + [jnp.zeros((128 - groups, seg), jnp.float32)], axis=0)
    shift_rows = jnp.concatenate(
        [shift_rows, jnp.zeros((128, 256 - seg), jnp.float32)], axis=1)
    shift_cols[...] = shift_rows.T

    for n, (cols, trio) in enumerate(copies):
        for copy in trio:
            copy.wait()
        wide = tok_ref[:, :, cols].reshape(rows, chunks[n]).astype(jnp.float32)
        new = new_ref[:, cols].astype(jnp.float32)
        new = jnp.concatenate([new, jnp.zeros((pad - seqs, chunks[n]), jnp.float32)], axis=0)
        wide = jnp.concatenate([wide, new], axis=0)
        squares = wide * wide
        part = squares[:, 0:128]
        for c in range(1, chunks[n] // 128):
            part = part + squares[:, c * 128 : (c + 1) * 128]
        x = (wide * gain_ref[:, cols]).astype(jnp.bfloat16)
        yf = jnp.dot(x, wf_ref[cols, :], preferred_element_type=jnp.float32)
        yv = jnp.dot(x, wv_ref[cols, :], preferred_element_type=jnp.float32)
        if n == 0:
            accf[...] = yf
            accv[...] = yv
            ssq[...] = part
        else:
            accf[...] += yf
            accv[...] += yv
            ssq[...] += part

    gap_row = jnp.concatenate([gap_ref[h : h + 1, :] for h in range(heads)], axis=1)
    ti = lax.broadcasted_iota(jnp.int32, (seg, seg), 0)
    tj = lax.broadcasted_iota(jnp.int32, (seg, seg), 1)
    later = (tj > ti).astype(jnp.float32).astype(jnp.bfloat16)
    total_rows = []
    for s in range(seqs):
        here = slice(s * seg, (s + 1) * seg)
        scale = lax.rsqrt(
            jnp.sum(ssq[here, :], axis=1, keepdims=True) / model_width + epsilon)
        key_gate = gap_row * jax.nn.sigmoid(-(accf[here, :] * scale))
        shift = jnp.concatenate(
            [jnp.broadcast_to(shift_cols[0:seg, s * heads + h : s * heads + h + 1],
                              (seg, key_dim)) for h in range(heads)], axis=1)
        log_forget = jnp.log1p(-key_gate) + shift
        high = log_forget.astype(jnp.bfloat16)
        low = (log_forget - high.astype(jnp.float32)).astype(jnp.bfloat16)
        within = jnp.dot(later, high, preferred_element_type=jnp.float32)
        within = within + jnp.dot(later, low, preferred_element_type=jnp.float32)
        weights = (key_gate * jnp.exp(within)).astype(jnp.bfloat16)
        values = (accv[here, :] * scale).astype(jnp.bfloat16)
        total = jnp.sum(log_forget, axis=0, keepdims=True)
        for h in range(heads):
            lanes = slice(h * key_dim, (h + 1) * key_dim)
            group = s * heads + h
            total_rows.append(total[:, lanes])
            pieces[...] = lax.dot_general(
                weights[:, lanes], values[:, lanes], (((0,), (0,)), ((), ())),
                preferred_element_type=jnp.float32)
            for i in range(per):
                buf_ref[pl.ds(i * groups + group, devices, stride=rank), :] = (
                    pieces[pl.ds(i, devices, stride=per), :])
    totals = jnp.concatenate(
        total_rows + [jnp.zeros((128 - groups, key_dim), jnp.float32)], axis=0)
    total_cols[...] = totals.T
    packed = total_cols[pl.ds(0, devices, stride=per), :]
    for i in range(1, per):
        packed = packed + pltpu.roll(
            total_cols[pl.ds(i, devices, stride=per), :], i * groups, 1)
    buf_ref[pl.ds(STATE_ROWS, devices, stride=rank), :] = packed
    for extra in range(STATE_ROWS + 1, rank):
        buf_ref[pl.ds(extra, devices, stride=rank), :] = jnp.zeros_like(packed)

    last = slice(rows, rows + pad)
    scale = lax.rsqrt(
        jnp.sum(ssq[last, :], axis=1, keepdims=True) / model_width + epsilon)
    new_key = gap_row * jax.nn.sigmoid(-(accf[last, :] * scale))
    new_values = (accv[last, :] * scale).astype(jnp.bfloat16).astype(jnp.float32)
    for h in range(heads):
        lanes = slice(h * key_dim, (h + 1) * key_dim)
        nk_ref[pl.ds(h, seqs, stride=heads), :] = new_key[0:seqs, lanes]
        nv_ref[pl.ds(h, seqs, stride=heads), :] = new_values[0:seqs, lanes]


def settle_kernel(
    devices, per,
    place_ref, got_ref, nk_ref, nv_ref, query_ref,
    cache_ref, part_ref, state_ref,
):
    groups = nk_ref.shape[0]
    totals = got_ref[pl.ds(STATE_ROWS, devices, stride=BLOCK_ROWS), :]
    cols = jnp.concatenate(
        [totals, jnp.zeros((128 - devices, 128), jnp.float32)], axis=0).T[0:STATE_ROWS]
    later = pltpu.roll(cols, 127, 1)
    reach = 1
    while reach < devices:
        later = later + pltpu.roll(later, 128 - reach, 1)
        reach *= 2
    factor = jnp.exp(later)
    lane = lax.broadcasted_iota(jnp.int32, (groups, 128), 1)
    first = place_ref[0] * per
    query = jnp.concatenate(
        [query_ref[s].astype(jnp.float32) for s in range(query_ref.shape[0])], axis=0)
    part = jnp.zeros((groups, 128), jnp.float32)
    for i in range(per):
        base = i * groups
        state = factor[base : base + groups, 0:1] * got_ref[base : base + groups, :]
        for g in range(1, devices):
            start = g * BLOCK_ROWS + base
            state = state + factor[base : base + groups, g : g + 1] * got_ref[
                start : start + groups, :]
        state_ref[pl.ds(i, groups, stride=per), :] = state
        new_key = jnp.sum(
            jnp.where(lane == first + i, nk_ref[...], 0.0), axis=1, keepdims=True)
        updated = (1.0 - new_key) * state + new_key * nv_ref[...]
        part = part + query[:, i : i + 1] * updated
    cache_ref[...] = state_ref[...].astype(jnp.bfloat16)
    for d in range(devices):
        part_ref[d * groups : (d + 1) * groups, :] = part


def read_kernel(devices, got_ref, gain_ref, read_ref):
    seqs, heads, val_dim = read_ref.shape
    groups = seqs * heads
    raw = got_ref[0:groups, :]
    for d in range(1, devices):
        raw = raw + got_ref[d * groups : (d + 1) * groups, :]
    gain = jnp.concatenate([gain_ref[...]] * seqs, axis=0)
    mean = jnp.sum(raw * raw, axis=1, keepdims=True) / val_dim
    out = raw * lax.rsqrt(mean + epsilon) * gain
    for s in range(seqs):
        read_ref[s] = out[s * heads : (s + 1) * heads, :]


def segments(tokens, new_tokens, gain_row, w_forget, w_value, gap, shift_rows):
    seqs, seg, model_width = tokens.shape
    heads, key_dim = gap.shape
    width = w_forget.shape[1]
    val_dim = width // heads
    groups = seqs * heads
    devices = key_dim * groups // STATE_ROWS
    rows = seqs * seg + 16
    f32 = jnp.float32
    whole = pl.BlockSpec(memory_space=pltpu.VMEM)
    hbm = pl.BlockSpec(memory_space=pltpu.HBM)
    return pl.pallas_call(
        functools.partial(segment_kernel, seqs, heads, key_dim, CHUNKS),
        in_specs=[hbm] * 7,
        out_specs=[whole, whole, whole],
        out_shape=[
            jax.ShapeDtypeStruct((devices * BLOCK_ROWS, val_dim), f32),
            jax.ShapeDtypeStruct((groups, key_dim), f32),
            jax.ShapeDtypeStruct((groups, val_dim), f32),
        ],
        scratch_shapes=[
            pltpu.VMEM((seqs, seg, model_width), jnp.bfloat16),
            pltpu.VMEM((model_width, width), jnp.bfloat16),
            pltpu.VMEM((model_width, width), jnp.bfloat16),
            pltpu.VMEM((seqs, model_width), jnp.bfloat16),
            pltpu.VMEM((1, model_width), f32),
            pltpu.VMEM((heads, key_dim), f32),
            pltpu.VMEM((seqs, heads, seg), f32),
            pltpu.VMEM((rows, width), f32),
            pltpu.VMEM((rows, width), f32),
            pltpu.VMEM((rows, 128), f32),
            pltpu.VMEM((key_dim, val_dim), f32),
            pltpu.VMEM((256, 128), f32),
            pltpu.VMEM((128, 128), f32),
            pltpu.SemaphoreType.DMA((4, max(4, len(CHUNKS)))),
        ],
        compiler_params=pltpu.CompilerParams(vmem_limit_bytes=VMEM_MIB * 2**20),
        name="segment",
    )(
        *(pltpu.with_memory_space_constraint(x, pltpu.HBM) for x in (
            tokens, new_tokens, gain_row, w_forget, w_value, gap, shift_rows))
    )


def local(tokens, new_tokens, in_gain, w_forget, w_value, gap, decay_shift, query, out_gain):
    seqs, seg, model_width = tokens.shape
    heads, key_dim = gap.shape
    val_dim = out_gain.shape[1]
    devices = lax.axis_size("sp")
    per = key_dim // devices
    groups = seqs * heads
    whole = pl.BlockSpec(memory_space=pltpu.VMEM)
    f32 = jnp.float32
    buf, new_key, new_values = segments(
        tokens, new_tokens, in_gain.reshape(1, model_width), w_forget, w_value, gap,
        jnp.transpose(decay_shift, (0, 2, 1)))
    got = lax.all_to_all(
        buf.reshape(devices, BLOCK_ROWS, 1, val_dim), "sp", 0, 0, tiled=True
    ).reshape(devices * BLOCK_ROWS, val_dim)
    place = lax.axis_index("sp").astype(jnp.int32).reshape(1)
    cache, part = pl.pallas_call(
        functools.partial(settle_kernel, devices, per),
        in_specs=[pl.BlockSpec(memory_space=pltpu.SMEM), whole, whole, whole, whole],
        out_specs=[whole, whole],
        out_shape=[
            jax.ShapeDtypeStruct((STATE_ROWS, val_dim), jnp.bfloat16),
            jax.ShapeDtypeStruct((devices * groups, val_dim), f32),
        ],
        scratch_shapes=[pltpu.VMEM((STATE_ROWS, val_dim), f32)],
        compiler_params=pltpu.CompilerParams(vmem_limit_bytes=8 * 2**20),
        name="settle",
    )(place, got, new_key, new_values, query)
    everything = lax.all_to_all(
        part.reshape(devices, groups, val_dim), "sp", 0, 0, tiled=True
    ).reshape(devices * groups, val_dim)
    read = pl.pallas_call(
        functools.partial(read_kernel, devices),
        in_specs=[whole, whole],
        out_specs=whole,
        out_shape=jax.ShapeDtypeStruct((seqs, heads, val_dim), f32),
        compiler_params=pltpu.CompilerParams(vmem_limit_bytes=8 * 2**20),
        name="read",
    )(everything, out_gain)
    return (cache.reshape(seqs, heads, per, val_dim), read)


def solution(mesh):
    return jax.shard_map(
        local,
        mesh=mesh,
        in_specs=(
            P("gr", "sp", None),
            P("gr", None),
            P(),
            P(None, "tp"),
            P(None, "tp"),
            P("tp", None),
            P("gr", "sp", "tp"),
            P("gr", "tp", "sp"),
            P("tp", None),
        ),
        out_specs=(P("gr", "tp", "sp", None), P("gr", "tp", None)),
        check_vma=False,
    )
```

time: 62.8 us -> 56.8 us (0.904)
  blocking collectives: 0 us -> 15.8 us
  waiting for transfers between devices: 26.9 us -> 17 us
  starting transfers between devices: 18.4 us -> 12.9 us
  Pallas kernels: 14.4 us -> 10.2 us
  local copies, waits for them, and re-layouts: 1.38 us -> 0.01 us
    all_to_all x0 -> x1, blocking collectives: none -> 15.8 us  [local(): lax.all_to_all(part.reshape(devices, groups, val_dim), 'sp', 0, 0, tiled=...]
    all_to_all x1 -> x0, waiting for transfers between devices: 9.89 us -> none  [local(): lax.all_to_all(part.reshape(devices, groups, val_dim), 'sp', 0, 0, tiled=...]
    all_to_all x1 -> x0, starting transfers between devices: 5.49 us -> none  [local(): lax.all_to_all(part.reshape(devices, groups, val_dim), 'sp', 0, 0, tiled=...]
    pallas_call x1, Pallas kernels: 12.3 us -> 8.15 us  [segments(): pl.pallas_call(functools.partial(segment_kernel, seqs, heads, key_dim, CH...]
    unnamed x8 -> x4, local copies, waits for them, and re-layouts: 1.38 us -> 0.01 us
  transfers between devices with their start and end apart: 2 -> 1, of which waited for: 2 -> 1; matrix products, arithmetic and copies ran while one was open for 1% -> 0% of each run, Pallas kernels for 0% -> 0%
where the time goes in v2:
time: 56.8 us; the launch traced here: 56.6 us
  waiting for transfers between devices  17 us (30%)
  blocking collectives  15.8 us (28%)
  starting transfers between devices  12.9 us (23%)
  Pallas kernels  10.2 us (18%)
  between operations  0.67 us (1%)
    all_to_all x1, waiting for transfers between devices, local(): lax.all_to_all(buf.reshape(devices, BLOCK_ROWS, 1, val_dim), 'sp', 0, 0,...  17 us
    all_to_all x1, blocking collectives, local(): lax.all_to_all(part.reshape(devices, groups, val_dim), 'sp', 0, 0, tiled=...  15.8 us
    all_to_all x1, starting transfers between devices, local(): lax.all_to_all(buf.reshape(devices, BLOCK_ROWS, 1, val_dim), 'sp', 0, 0,...  12.9 us
    pallas_call x1, Pallas kernels, segments(): pl.pallas_call(functools.partial(segment_kernel, seqs, heads, key_dim, CH...  8.15 us
    pallas_call x1, Pallas kernels, local(): pl.pallas_call(functools.partial(settle_kernel, devices, per), in_specs=[...  1.36 us
  transfers between devices with their start and end apart: 1, of which 1 were waited for; matrix products, arithmetic and copies ran while one was open for 0% of the time, Pallas kernels for 0%

profile of v2, /device:TPU:6, one launch (start us, length us, event | category | flops | bytes accessed | tf_op | source)
XLA Modules:
  0.0 56.6 jit_solution(5402383698600636616)
XLA Ops:
  0.6 0.0 copy-start
  0.6 0.0 copy-start.1
  0.7 8.2 %segment.1 = (f32[1056,128]{1,0:T(8,128)}, f32[8,128]{1,0:T(8,128)S(1)}, f32[8,128]{1,0:T(8,128)S(1)}) custom-call(bf16[4,192,4096]{2,1,0:T(8,128)(2,1)} %tok_hbm.1, bf16[4,4096]{1,0:T(4,128)(2,1)} %new_hbm.1, f32[1,4096]{1,0:T(1,128)} %bitcast.11, bf16[4096,256]{1,0:T(8,128)(2,1)} %wf_hbm.1, bf16[4096,256]{1,0:T(8,128)(2,1)} %wv_hbm.1, f32[2,128]{1,0:T(2,128)} %gap_hbm.1, ...), custom_call_target="tpu_custom_call" | custom-call | tf_op jit(solution)/shard_map/segment/pallas_call | solution.py:201
  8.8 12.9 %all-to-all-start = ((f32[32,33,1,128]{3,2,1,0:T(1,128)}), f32[32,33,1,128]{3,2,1,0:T(1,128)S(1)}, u32[]{:S(2)}, u32[]{:S(2)}) async-start(f32[32,33,1,128]{3,2,1,0:T(1,128)} %bitcast.3), calls=%async_computation | async-start | bytes 1081344 | tf_op jit(solution)/shard_map/all_to_all | solution.py:246
  21.8 17.0 %all-to-all-done = f32[32,33,1,128]{3,2,1,0:T(1,128)S(1)} async-done(((f32[32,33,1,128]{3,2,1,0:T(1,128)}), f32[32,33,1,128]{3,2,1,0:T(1,128)S(1)}, u32[]{:S(2)}, u32[]{:S(2)}) %all-to-all-start) | async-done | bytes 540704 | tf_op jit(solution)/shard_map/all_to_all | solution.py:246
  38.7 0.0 copy-done
  38.7 1.4 %settle.1 = (bf16[32,128]{1,0:T(8,128)(2,1)}, f32[256,128]{1,0:T(8,128)S(1)}) custom-call(s32[1]{0:T(128)} %bitcast.place_ref, f32[1056,128]{1,0:T(8,128)S(1)} %bitcast.8, f32[8,128]{1,0:T(8,128)S(1)} %get-tuple-element.8.nk_ref, f32[8,128]{1,0:T(8,128)S(1)} %get-tuple-element.9.nv_ref, bf16[4,2,4]{2,1,0:T(2,128)(2,1)S(1)} %copy-done), custom_call_target="tpu_custom_call" | custom-call | tf_op jit(solution)/shard_map/settle/pallas_call | solution.py:250
  40.1 15.8 %all_to_all.10 = f32[32,8,128]{2,1,0:T(8,128)S(1)} all-to-all(f32[32,8,128]{2,1,0:T(8,128)S(1)} %bitcast.10), channel_id=1, replica_groups=mesh['gr'=3,'sp'=32,'tp'=8] {'sp'}, dimensions={0} | all-to-all | bytes 262144 | tf_op jit(solution)/shard_map/all_to_all | solution.py:262
  55.9 0.0 copy-done.1
  55.9 0.7 %read.1 = f32[4,2,128]{2,1,0:T(2,128)} custom-call(f32[256,128]{1,0:T(8,128)S(1)} %bitcast.9, f32[2,128]{1,0:T(2,128)S(1)} %copy-done.1), custom_call_target="tpu_custom_call" | custom-call | tf_op jit(solution)/shard_map/read/pallas_call | solution.py:265
Async XLA Ops:
  0.6 38.1 %copy-start = (bf16[4,2,4]{2,1,0:T(2,128)(2,1)S(1)}, bf16[4,2,4]{2,1,0:T(2,128)(2,1)}, u32[]{:S(2)}) copy-start(bf16[4,2,4]{2,1,0:T(2,128)(2,1)} %query_ref.1) | copy-start | bytes 196
  0.6 55.2 %copy-start.1 = (f32[2,128]{1,0:T(2,128)S(1)}, f32[2,128]{1,0:T(2,128)}, u32[]{:S(2)}) copy-start(f32[2,128]{1,0:T(2,128)} %gain_ref.1) | copy-start | bytes 3076
  8.8 29.9 %all-to-all-start = ((f32[32,33,1,128]{3,2,1,0:T(1,128)}), f32[32,33,1,128]{3,2,1,0:T(1,128)S(1)}, u32[]{:S(2)}, u32[]{:S(2)}) async-start(f32[32,33,1,128]{3,2,1,0:T(1,128)} %bitcast.3), calls=%async_computation | async-start | bytes 1081344 | tf_op jit(solution)/shard_map/all_to_all | solution.py:246

commit v3 on v2

--- a/solution.py
+++ b/solution.py
@@ -11,7 +11,7 @@
 
 STATE_ROWS = 32
 BLOCK_ROWS = 33
-CHUNKS = (512, 512, 1024, 1024, 1024)
+CHUNKS = (512,) * 8
 VMEM_MIB = 48
 
 
@@ -139,7 +139,7 @@
 
 def settle_kernel(
     devices, per,
-    place_ref, got_ref, nk_ref, nv_ref, query_ref,
+    got_ref, nk_ref, nv_ref, query_ref,
     cache_ref, part_ref, state_ref,
 ):
     groups = nk_ref.shape[0]
@@ -153,7 +153,7 @@
         reach *= 2
     factor = jnp.exp(later)
     lane = lax.broadcasted_iota(jnp.int32, (groups, 128), 1)
-    first = place_ref[0] * per
+    first = lax.axis_index("sp") * per
     query = jnp.concatenate(
         [query_ref[s].astype(jnp.float32) for s in range(query_ref.shape[0])], axis=0)
     part = jnp.zeros((groups, 128), jnp.float32)
@@ -174,8 +174,9 @@
         part_ref[d * groups : (d + 1) * groups, :] = part
 
 
-def read_kernel(devices, got_ref, gain_ref, read_ref):
+def read_kernel(devices, got_ref, gain_ref, state_ref, read_ref, cache_ref):
     seqs, heads, val_dim = read_ref.shape
+    cache_ref[...] = state_ref[...]
     groups = seqs * heads
     raw = got_ref[0:groups, :]
     for d in range(1, devices):
@@ -246,10 +247,9 @@
     got = lax.all_to_all(
         buf.reshape(devices, BLOCK_ROWS, 1, val_dim), "sp", 0, 0, tiled=True
     ).reshape(devices * BLOCK_ROWS, val_dim)
-    place = lax.axis_index("sp").astype(jnp.int32).reshape(1)
-    cache, part = pl.pallas_call(
+    state, part = pl.pallas_call(
         functools.partial(settle_kernel, devices, per),
-        in_specs=[pl.BlockSpec(memory_space=pltpu.SMEM), whole, whole, whole, whole],
+        in_specs=[whole, whole, whole, whole],
         out_specs=[whole, whole],
         out_shape=[
             jax.ShapeDtypeStruct((STATE_ROWS, val_dim), jnp.bfloat16),
@@ -258,18 +258,21 @@
         scratch_shapes=[pltpu.VMEM((STATE_ROWS, val_dim), f32)],
         compiler_params=pltpu.CompilerParams(vmem_limit_bytes=8 * 2**20),
         name="settle",
-    )(place, got, new_key, new_values, query)
+    )(got, new_key, new_values, query)
     everything = lax.all_to_all(
         part.reshape(devices, groups, val_dim), "sp", 0, 0, tiled=True
     ).reshape(devices * groups, val_dim)
-    read = pl.pallas_call(
+    read, cache = pl.pallas_call(
         functools.partial(read_kernel, devices),
-        in_specs=[whole, whole],
-        out_specs=whole,
-        out_shape=jax.ShapeDtypeStruct((seqs, heads, val_dim), f32),
+        in_specs=[whole, whole, whole],
+        out_specs=[whole, whole],
+        out_shape=[
+            jax.ShapeDtypeStruct((seqs, heads, val_dim), f32),
+            jax.ShapeDtypeStruct((STATE_ROWS, val_dim), jnp.bfloat16),
+        ],
         compiler_params=pltpu.CompilerParams(vmem_limit_bytes=8 * 2**20),
         name="read",
-    )(everything, out_gain)
+    )(everything, out_gain, state)
     return (cache.reshape(seqs, heads, per, val_dim), read)
 
 

time: 56.8 us -> 55.1 us (0.970)
  blocking collectives: 15.8 us -> 45.5 us
  waiting for transfers between devices: 17 us -> 0 us
  starting transfers between devices: 12.9 us -> 0 us
  Pallas kernels: 10.2 us -> 8.72 us
    all_to_all x0 -> x1, blocking collectives: none -> 29.7 us  [local(): lax.all_to_all(buf.reshape(devices, BLOCK_ROWS, 1, val_dim), 'sp', 0, 0,...]
    all_to_all x1 -> x0, waiting for transfers between devices: 17 us -> none  [local(): lax.all_to_all(buf.reshape(devices, BLOCK_ROWS, 1, val_dim), 'sp', 0, 0,...]
    all_to_all x1 -> x0, starting transfers between devices: 12.9 us -> none  [local(): lax.all_to_all(buf.reshape(devices, BLOCK_ROWS, 1, val_dim), 'sp', 0, 0,...]
    pallas_call x1, Pallas kernels: 8.15 us -> 7.23 us  [segments(): pl.pallas_call(functools.partial(segment_kernel, seqs, heads, key_dim, CH...]
    pallas_call x1, Pallas kernels: 1.36 us -> 0.78 us  [local(): pl.pallas_call(functools.partial(settle_kernel, devices, per), in_specs=[...]
  transfers between devices with their start and end apart: 1 -> 0, of which waited for: 1 -> 0; matrix products, arithmetic and copies ran while one was open for 0% -> 0% of each run, Pallas kernels for 0% -> 0%
where the time goes in v3:
time: 55.1 us; the launch traced here: 54.9 us
  blocking collectives  45.5 us (83%)
  Pallas kernels  8.72 us (16%)
  between operations  0.67 us (1%)
    all_to_all x1, blocking collectives, local(): lax.all_to_all(buf.reshape(devices, BLOCK_ROWS, 1, val_dim), 'sp', 0, 0,...  29.7 us
    all_to_all x1, blocking collectives, local(): lax.all_to_all(part.reshape(devices, groups, val_dim), 'sp', 0, 0, tiled=...  15.8 us
    pallas_call x1, Pallas kernels, segments(): pl.pallas_call(functools.partial(segment_kernel, seqs, heads, key_dim, CH...  7.23 us

profile of v3, /device:TPU:6, one launch (start us, length us, event | category | flops | bytes accessed | tf_op | source)
XLA Modules:
  0.0 54.9 jit_solution(6034280504191044634)
XLA Ops:
  0.6 0.0 copy-start
  0.6 0.0 copy-start.1
  0.7 7.2 %segment.1 = (f32[1056,128]{1,0:T(8,128)S(1)}, f32[8,128]{1,0:T(8,128)S(1)}, f32[8,128]{1,0:T(8,128)S(1)}) custom-call(bf16[4,192,4096]{2,1,0:T(8,128)(2,1)} %tok_hbm.1, bf16[4,4096]{1,0:T(4,128)(2,1)} %new_hbm.1, f32[1,4096]{1,0:T(1,128)} %bitcast.11, bf16[4096,256]{1,0:T(8,128)(2,1)} %wf_hbm.1, bf16[4096,256]{1,0:T(8,128)(2,1)} %wv_hbm.1, ...), custom_call_target="tpu_custom_call" | custom-call | tf_op jit(solution)/shard_map/segment/pallas_call | solution.py:202
  7.9 29.7 %all_to_all.10 = f32[32,33,1,128]{3,2,1,0:T(1,128)S(1)} all-to-all(f32[32,33,1,128]{3,2,1,0:T(1,128)S(1)} %bitcast.8), channel_id=1, replica_groups=mesh['gr'=3,'sp'=32,'tp'=8] {'sp'}, dimensions={0} | all-to-all | bytes 1081344 | tf_op jit(solution)/shard_map/all_to_all | solution.py:247
  37.6 0.0 copy-done
  37.6 0.8 %settle.1 = (bf16[32,128]{1,0:T(8,128)(2,1)S(1)}, f32[256,128]{1,0:T(8,128)S(1)}) custom-call(f32[1056,128]{1,0:T(8,128)S(1)} %bitcast.7, f32[8,128]{1,0:T(8,128)S(1)} %get-tuple-element.10.nk_ref, f32[8,128]{1,0:T(8,128)S(1)} %get-tuple-element.11.nv_ref, bf16[4,2,4]{2,1,0:T(2,128)(2,1)S(1)} %copy-done), custom_call_target="tpu_custom_call" | custom-call | tf_op jit(solution)/shard_map/settle/pallas_call | solution.py:250
  38.4 15.8 %all_to_all.11 = f32[32,8,128]{2,1,0:T(8,128)S(1)} all-to-all(f32[32,8,128]{2,1,0:T(8,128)S(1)} %bitcast.10), channel_id=1, replica_groups=mesh['gr'=3,'sp'=32,'tp'=8] {'sp'}, dimensions={0} | all-to-all | bytes 262144 | tf_op jit(solution)/shard_map/all_to_all | solution.py:262
  54.2 0.0 copy-done.1
  54.2 0.7 %read.1 = (f32[4,2,128]{2,1,0:T(2,128)}, bf16[32,128]{1,0:T(8,128)(2,1)}) custom-call(f32[256,128]{1,0:T(8,128)S(1)} %bitcast.9, f32[2,128]{1,0:T(2,128)S(1)} %copy-done.1, bf16[32,128]{1,0:T(8,128)(2,1)S(1)} %get-tuple-element.13.state_ref), custom_call_target="tpu_custom_call" | custom-call | tf_op jit(solution)/shard_map/read/pallas_call | solution.py:265
Async XLA Ops:
  0.6 37.0 %copy-start = (bf16[4,2,4]{2,1,0:T(2,128)(2,1)S(1)}, bf16[4,2,4]{2,1,0:T(2,128)(2,1)}, u32[]{:S(2)}) copy-start(bf16[4,2,4]{2,1,0:T(2,128)(2,1)} %query_ref.1) | copy-start | bytes 196
  0.6 53.5 %copy-start.1 = (f32[2,128]{1,0:T(2,128)S(1)}, f32[2,128]{1,0:T(2,128)}, u32[]{:S(2)}) copy-start(f32[2,128]{1,0:T(2,128)} %gain_ref.1) | copy-start | bytes 3076

commit v4 on v3

--- a/solution.py
+++ b/solution.py
@@ -19,7 +19,7 @@
     seqs, heads, key_dim, chunks,
     tok_hbm, new_hbm, gain_hbm, wf_hbm, wv_hbm, gap_hbm, shift_hbm,
     buf_ref, nk_ref, nv_ref,
-    tok_ref, wf_ref, wv_ref, new_ref, gain_ref, gap_ref, shift_ref, accf, accv, ssq, pieces, shift_cols, total_cols, sems,
+    tok_ref, wf_ref, wv_ref, new_ref, gain_ref, gap_ref, shift_ref, accf, accv, ssq, pieces, shift_cols, shift_wide, total_cols, sems,
 ):
     seg = tok_ref.shape[1]
     model_width = tok_ref.shape[2]
@@ -61,6 +61,9 @@
         [shift_rows, jnp.zeros((128, 256 - seg), jnp.float32)], axis=1)
     shift_cols[...] = shift_rows.T
 
+    widened = [[] for _ in chunks]
+    for s in range(seqs):
+        widened[min(s + 2, len(chunks) - 1)].append(s)
     for n, (cols, trio) in enumerate(copies):
         for copy in trio:
             copy.wait()
@@ -83,21 +86,24 @@
             accf[...] += yf
             accv[...] += yv
             ssq[...] += part
+        for s in widened[n]:
+            for h in range(heads):
+                group = s * heads + h
+                shift_wide[s * seg : (s + 1) * seg, h * key_dim : (h + 1) * key_dim] = (
+                    jnp.broadcast_to(shift_cols[0:seg, group : group + 1], (seg, key_dim)))
 
     gap_row = jnp.concatenate([gap_ref[h : h + 1, :] for h in range(heads)], axis=1)
     ti = lax.broadcasted_iota(jnp.int32, (seg, seg), 0)
     tj = lax.broadcasted_iota(jnp.int32, (seg, seg), 1)
     later = (tj > ti).astype(jnp.float32).astype(jnp.bfloat16)
     total_rows = []
+    gated = []
     for s in range(seqs):
         here = slice(s * seg, (s + 1) * seg)
         scale = lax.rsqrt(
             jnp.sum(ssq[here, :], axis=1, keepdims=True) / model_width + epsilon)
         key_gate = gap_row * jax.nn.sigmoid(-(accf[here, :] * scale))
-        shift = jnp.concatenate(
-            [jnp.broadcast_to(shift_cols[0:seg, s * heads + h : s * heads + h + 1],
-                              (seg, key_dim)) for h in range(heads)], axis=1)
-        log_forget = jnp.log1p(-key_gate) + shift
+        log_forget = jnp.log1p(-key_gate) + shift_wide[here, :]
         high = log_forget.astype(jnp.bfloat16)
         low = (log_forget - high.astype(jnp.float32)).astype(jnp.bfloat16)
         within = jnp.dot(later, high, preferred_element_type=jnp.float32)
@@ -109,12 +115,14 @@
             lanes = slice(h * key_dim, (h + 1) * key_dim)
             group = s * heads + h
             total_rows.append(total[:, lanes])
-            pieces[...] = lax.dot_general(
-                weights[:, lanes], values[:, lanes], (((0,), (0,)), ((), ())),
-                preferred_element_type=jnp.float32)
-            for i in range(per):
-                buf_ref[pl.ds(i * groups + group, devices, stride=rank), :] = (
-                    pieces[pl.ds(i, devices, stride=per), :])
+            gated.append((weights[:, lanes], values[:, lanes]))
+    for group in range(groups):
+        pieces[group] = lax.dot_general(
+            *gated[group], (((0,), (0,)), ((), ())), preferred_element_type=jnp.float32)
+    for group in range(groups):
+        for i in range(per):
+            buf_ref[pl.ds(i * groups + group, devices, stride=rank), :] = (
+                pieces[group, pl.ds(i, devices, stride=per), :])
     totals = jnp.concatenate(
         total_rows + [jnp.zeros((128 - groups, key_dim), jnp.float32)], axis=0)
     total_cols[...] = totals.T
@@ -219,8 +227,9 @@
             pltpu.VMEM((rows, width), f32),
             pltpu.VMEM((rows, width), f32),
             pltpu.VMEM((rows, 128), f32),
-            pltpu.VMEM((key_dim, val_dim), f32),
+            pltpu.VMEM((groups, key_dim, val_dim), f32),
             pltpu.VMEM((256, 128), f32),
+            pltpu.VMEM((seqs * seg, width), f32),
             pltpu.VMEM((128, 128), f32),
             pltpu.SemaphoreType.DMA((4, max(4, len(CHUNKS)))),
         ],

time: 55.1 us -> 54.3 us (0.985)
  Pallas kernels: 8.72 us -> 7.97 us
    pallas_call x1, Pallas kernels: 7.23 us -> 6.48 us  [segments(): pl.pallas_call(functools.partial(segment_kernel, seqs, heads, key_dim, CH...]
where the time goes in v4:
time: 54.3 us; the launch traced here: 54.1 us
  blocking collectives  45.5 us (84%)
  Pallas kernels  7.97 us (15%)
  between operations  0.67 us (1%)
    all_to_all x1, blocking collectives, local(): lax.all_to_all(buf.reshape(devices, BLOCK_ROWS, 1, val_dim), 'sp', 0, 0,...  29.7 us
    all_to_all x1, blocking collectives, local(): lax.all_to_all(part.reshape(devices, groups, val_dim), 'sp', 0, 0, tiled=...  15.8 us
    pallas_call x1, Pallas kernels, segments(): pl.pallas_call(functools.partial(segment_kernel, seqs, heads, key_dim, CH...  6.48 us

profile of v4, /device:TPU:6, one launch (start us, length us, event | category | flops | bytes accessed | tf_op | source)
XLA Modules:
  0.0 54.1 jit_solution(1404347674630813989)
XLA Ops:
  0.6 0.0 copy-start
  0.6 0.0 copy-start.1
  0.7 6.5 %segment.1 = (f32[1056,128]{1,0:T(8,128)S(1)}, f32[8,128]{1,0:T(8,128)S(1)}, f32[8,128]{1,0:T(8,128)S(1)}) custom-call(bf16[4,192,4096]{2,1,0:T(8,128)(2,1)} %tok_hbm.1, bf16[4,4096]{1,0:T(4,128)(2,1)} %new_hbm.1, f32[1,4096]{1,0:T(1,128)} %bitcast.11, bf16[4096,256]{1,0:T(8,128)(2,1)} %wf_hbm.1, bf16[4096,256]{1,0:T(8,128)(2,1)} %wv_hbm.1, ...), custom_call_target="tpu_custom_call" | custom-call | tf_op jit(solution)/shard_map/segment/pallas_call | solution.py:210
  7.1 29.7 %all_to_all.10 = f32[32,33,1,128]{3,2,1,0:T(1,128)S(1)} all-to-all(f32[32,33,1,128]{3,2,1,0:T(1,128)S(1)} %bitcast.8), channel_id=1, replica_groups=mesh['gr'=3,'sp'=32,'tp'=8] {'sp'}, dimensions={0} | all-to-all | bytes 1081344 | tf_op jit(solution)/shard_map/all_to_all | solution.py:256
  36.9 0.0 copy-done
  36.9 0.8 %settle.1 = (bf16[32,128]{1,0:T(8,128)(2,1)S(1)}, f32[256,128]{1,0:T(8,128)S(1)}) custom-call(f32[1056,128]{1,0:T(8,128)S(1)} %bitcast.7, f32[8,128]{1,0:T(8,128)S(1)} %get-tuple-element.10.nk_ref, f32[8,128]{1,0:T(8,128)S(1)} %get-tuple-element.11.nv_ref, bf16[4,2,4]{2,1,0:T(2,128)(2,1)S(1)} %copy-done), custom_call_target="tpu_custom_call" | custom-call | tf_op jit(solution)/shard_map/settle/pallas_call | solution.py:259
  37.6 15.8 %all_to_all.11 = f32[32,8,128]{2,1,0:T(8,128)S(1)} all-to-all(f32[32,8,128]{2,1,0:T(8,128)S(1)} %bitcast.10), channel_id=1, replica_groups=mesh['gr'=3,'sp'=32,'tp'=8] {'sp'}, dimensions={0} | all-to-all | bytes 262144 | tf_op jit(solution)/shard_map/all_to_all | solution.py:271
  53.4 0.0 copy-done.1
  53.4 0.7 %read.1 = (f32[4,2,128]{2,1,0:T(2,128)}, bf16[32,128]{1,0:T(8,128)(2,1)}) custom-call(f32[256,128]{1,0:T(8,128)S(1)} %bitcast.9, f32[2,128]{1,0:T(2,128)S(1)} %copy-done.1, bf16[32,128]{1,0:T(8,128)(2,1)S(1)} %get-tuple-element.13.state_ref), custom_call_target="tpu_custom_call" | custom-call | tf_op jit(solution)/shard_map/read/pallas_call | solution.py:274
Async XLA Ops:
  0.6 36.2 %copy-start = (bf16[4,2,4]{2,1,0:T(2,128)(2,1)S(1)}, bf16[4,2,4]{2,1,0:T(2,128)(2,1)}, u32[]{:S(2)}) copy-start(bf16[4,2,4]{2,1,0:T(2,128)(2,1)} %query_ref.1) | copy-start | bytes 196
  0.6 52.8 %copy-start.1 = (f32[2,128]{1,0:T(2,128)S(1)}, f32[2,128]{1,0:T(2,128)}, u32[]{:S(2)}) copy-start(f32[2,128]{1,0:T(2,128)} %gain_ref.1) | copy-start | bytes 3076

commit v5 on v4

--- a/solution.py
+++ b/solution.py
@@ -152,14 +152,15 @@
 ):
     groups = nk_ref.shape[0]
     totals = got_ref[pl.ds(STATE_ROWS, devices, stride=BLOCK_ROWS), :]
-    cols = jnp.concatenate(
-        [totals, jnp.zeros((128 - devices, 128), jnp.float32)], axis=0).T[0:STATE_ROWS]
-    later = pltpu.roll(cols, 127, 1)
-    reach = 1
-    while reach < devices:
-        later = later + pltpu.roll(later, 128 - reach, 1)
-        reach *= 2
-    factor = jnp.exp(later)
+    own = lax.broadcasted_iota(jnp.int32, (devices, devices), 0)
+    other = lax.broadcasted_iota(jnp.int32, (devices, devices), 1)
+    after = (other > own).astype(jnp.float32).astype(jnp.bfloat16)
+    later = jnp.zeros_like(totals)
+    for _ in range(3):
+        part = totals.astype(jnp.bfloat16)
+        later = later + jnp.dot(after, part, preferred_element_type=jnp.float32)
+        totals = totals - part.astype(jnp.float32)
+    factor = jnp.exp(later).T[0:STATE_ROWS]
     lane = lax.broadcasted_iota(jnp.int32, (groups, 128), 1)
     first = lax.axis_index("sp") * per
     query = jnp.concatenate(
@@ -186,9 +187,10 @@
     seqs, heads, val_dim = read_ref.shape
     cache_ref[...] = state_ref[...]
     groups = seqs * heads
-    raw = got_ref[0:groups, :]
-    for d in range(1, devices):
-        raw = raw + got_ref[d * groups : (d + 1) * groups, :]
+    sums = [got_ref[d * groups : (d + 1) * groups, :] for d in range(devices)]
+    while len(sums) > 1:
+        sums = [a + b for a, b in zip(sums[0::2], sums[1::2])] + sums[len(sums) // 2 * 2 :]
+    raw = sums[0]
     gain = jnp.concatenate([gain_ref[...]] * seqs, axis=0)
     mean = jnp.sum(raw * raw, axis=1, keepdims=True) / val_dim
     out = raw * lax.rsqrt(mean + epsilon) * gain

time: 54.3 us -> 54.1 us (level)
  no operation moved by 1% of the time
where the time goes in v5:
time: 54.1 us; the launch traced here: 53.9 us
  blocking collectives  45.5 us (84%)
  Pallas kernels  7.73 us (14%)
  between operations  0.67 us (1%)
    all_to_all x1, blocking collectives, local(): lax.all_to_all(buf.reshape(devices, BLOCK_ROWS, 1, val_dim), 'sp', 0, 0,...  29.7 us
    all_to_all x1, blocking collectives, local(): lax.all_to_all(part.reshape(devices, groups, val_dim), 'sp', 0, 0, tiled=...  15.8 us
    pallas_call x1, Pallas kernels, segments(): pl.pallas_call(functools.partial(segment_kernel, seqs, heads, key_dim, CH...  6.48 us

profile of v5, /device:TPU:6, one launch (start us, length us, event | category | flops | bytes accessed | tf_op | source)
XLA Modules:
  0.0 53.9 jit_solution(7294541491810393468)
XLA Ops:
  0.6 0.0 copy-start
  0.6 0.0 copy-start.1
  0.7 6.5 %segment.1 = (f32[1056,128]{1,0:T(8,128)S(1)}, f32[8,128]{1,0:T(8,128)S(1)}, f32[8,128]{1,0:T(8,128)S(1)}) custom-call(bf16[4,192,4096]{2,1,0:T(8,128)(2,1)} %tok_hbm.1, bf16[4,4096]{1,0:T(4,128)(2,1)} %new_hbm.1, f32[1,4096]{1,0:T(1,128)} %bitcast.11, bf16[4096,256]{1,0:T(8,128)(2,1)} %wf_hbm.1, bf16[4096,256]{1,0:T(8,128)(2,1)} %wv_hbm.1, ...), custom_call_target="tpu_custom_call" | custom-call | tf_op jit(solution)/shard_map/segment/pallas_call | solution.py:212
  7.1 29.7 %all_to_all.10 = f32[32,33,1,128]{3,2,1,0:T(1,128)S(1)} all-to-all(f32[32,33,1,128]{3,2,1,0:T(1,128)S(1)} %bitcast.8), channel_id=1, replica_groups=mesh['gr'=3,'sp'=32,'tp'=8] {'sp'}, dimensions={0} | all-to-all | bytes 1081344 | tf_op jit(solution)/shard_map/all_to_all | solution.py:258
  36.9 0.0 copy-done
  36.9 0.6 %settle.1 = (bf16[32,128]{1,0:T(8,128)(2,1)S(1)}, f32[256,128]{1,0:T(8,128)S(1)}) custom-call(f32[1056,128]{1,0:T(8,128)S(1)} %bitcast.7, f32[8,128]{1,0:T(8,128)S(1)} %get-tuple-element.10.nk_ref, f32[8,128]{1,0:T(8,128)S(1)} %get-tuple-element.11.nv_ref, bf16[4,2,4]{2,1,0:T(2,128)(2,1)S(1)} %copy-done), custom_call_target="tpu_custom_call" | custom-call | tf_op jit(solution)/shard_map/settle/pallas_call | solution.py:261
  37.4 15.8 %all_to_all.11 = f32[32,8,128]{2,1,0:T(8,128)S(1)} all-to-all(f32[32,8,128]{2,1,0:T(8,128)S(1)} %bitcast.10), channel_id=1, replica_groups=mesh['gr'=3,'sp'=32,'tp'=8] {'sp'}, dimensions={0} | all-to-all | bytes 262144 | tf_op jit(solution)/shard_map/all_to_all | solution.py:273
  53.2 0.0 copy-done.1
  53.2 0.7 %read.1 = (f32[4,2,128]{2,1,0:T(2,128)}, bf16[32,128]{1,0:T(8,128)(2,1)}) custom-call(f32[256,128]{1,0:T(8,128)S(1)} %bitcast.9, f32[2,128]{1,0:T(2,128)S(1)} %copy-done.1, bf16[32,128]{1,0:T(8,128)(2,1)S(1)} %get-tuple-element.13.state_ref), custom_call_target="tpu_custom_call" | custom-call | tf_op jit(solution)/shard_map/read/pallas_call | solution.py:276
Async XLA Ops:
  0.6 36.2 %copy-start = (bf16[4,2,4]{2,1,0:T(2,128)(2,1)S(1)}, bf16[4,2,4]{2,1,0:T(2,128)(2,1)}, u32[]{:S(2)}) copy-start(bf16[4,2,4]{2,1,0:T(2,128)(2,1)} %query_ref.1) | copy-start | bytes 196
  0.6 52.6 %copy-start.1 = (f32[2,128]{1,0:T(2,128)S(1)}, f32[2,128]{1,0:T(2,128)}, u32[]{:S(2)}) copy-start(f32[2,128]{1,0:T(2,128)} %gain_ref.1) | copy-start | bytes 3076
